TPU v7x, 32 devices: a whole 2x2x4 slice. The times are simulated.
32 devices in a mesh: sp: 8 (over z, y), tp: 4 (over x, core).
Axes of the slice: x: 2, y: 2, z: 4, core: 2. Of those that a mesh axis runs over, the one named last changes fastest.
Arguments:
- residual_entry_input: bfloat16 [8192, 2048], P(('sp', 'tp')), may hold values from -6 to 6
- query_matrix_rows: bfloat16 [8192, 1024], P('sp', 'tp'), may hold values from -6 to 6
- key_matrix_rows: bfloat16 [8192, 1024], P('sp', 'tp'), may hold values from -6 to 6
- value_matrix_rows: bfloat16 [8192, 2048], P('sp', 'tp'), may hold values from -6 to 6
- output_gate_logits: bfloat16 [8192, 2048], P('sp', 'tp'), may hold values from -6 to 6
- input_gate_logits: float32 [8192, 8], P('sp', 'tp'), may hold values from -6 to 6
- forget_gate_logits: float32 [8192, 8], P('sp', 'tp'), may hold values from -8 to 31
- forget_decay_offset: float32 [8192, 8], P('sp', 'tp'), may hold values from -0.7 to 0
- head_norm_gain: float32 [8, 256], P('tp'), may hold values from 0.1 to 1.9
- cell_output_weight: bfloat16 [2048, 2048], P('tp'), may hold values from -0.125 to 0.125
- feedforward_norm_gain: float32 [2048], replicated, may hold values from 0.1 to 1.9
- gate_up_weight: bfloat16 [2048, 5632], P('sp', 'tp'), may hold values from -0.125 to 0.125
- value_up_weight: bfloat16 [2048, 5632], P('sp', 'tp'), may hold values from -0.125 to 0.125
- gate_filter_taps: float32 [3, 5632], P(None, 'tp'), may hold values from -3 to 3
- value_filter_taps: float32 [3, 5632], P(None, 'tp'), may hold values from -3 to 3
- down_projection_weight: bfloat16 [5632, 2048], P('tp', 'sp'), may hold values from -0.078125 to 0.078125
Outputs:
- result: bfloat16 [8192, 2048], P(('sp', 'tp'))
All inputs are finite; a program needn't handle non-finite values.
Results may differ from a plain program's by a relative error of at most 0.025.
Values may be sent and summed in bfloat16 or wider, within the bound.
No kernel may reach another device: no remote copies, remote signals or barrier semaphores. Data moves between devices by JAX's collectives and lax.ppermute only.
A program may use at most 128 MiB of HBM per device.

v0:
```python
import jax
import jax.numpy as jnp
from jax import lax
from jax.sharding import PartitionSpec as P

BLOCK = 128
eps = 1e-06
neg_large = -1e30


def carried_in(x, axis, combine, identity):
    count, position = (lax.axis_size(axis), lax.axis_index(axis))
    everything = jax.tree.map(
        lambda part, kind: lax.all_gather(part.astype(kind), axis),
        x,
        (jnp.bfloat16, jnp.bfloat16, jnp.bfloat16, jnp.bfloat16),
    )
    start = jax.tree.map(
        lambda part, zero: jnp.broadcast_to(jnp.asarray(zero, part.dtype), part.shape), x, identity
    )

    def lap(k, before):
        reached = k < position
        new = combine(
            before, jax.tree.map(lambda part, own: part[k].astype(own.dtype), everything, x)
        )
        return jax.tree.map(lambda a, b: jnp.where(reached, a, b), new, before)

    return lax.fori_loop(0, count, lap, start)


def shifted(x, axis, by):
    count = lax.axis_size(axis)
    pairs = [(i, i + by) for i in range(count) if 0 <= i + by < count]
    return lax.ppermute(x, axis, pairs)


def gate_log_values(input_gate_logits, forget_gate_logits, forget_decay_offset):
    input_log_value = 15.0 * jnp.tanh(input_gate_logits / 15.0)
    forget_log_sigmoid = (
        jax.nn.log_sigmoid(15.0 * jnp.tanh(forget_gate_logits / 15.0)) + forget_decay_offset
    )
    return (input_log_value, forget_log_sigmoid)


def combine_states(earlier, later):
    total_one, memory_one, normer_one, running_one = earlier
    total_two, memory_two, normer_two, running_two = later
    joined = jnp.maximum(total_two + running_one, running_two)
    weight_one = jnp.exp(total_two + running_one - joined)
    weight_two = jnp.exp(running_two - joined)
    memory = weight_one[:, None, None] * memory_one + weight_two[:, None, None] * memory_two
    normer = weight_one[:, None] * normer_one + weight_two[:, None] * normer_two
    return (total_one + total_two, memory, normer, joined)


def local_step(state_carry, inputs):
    memory, normer, running = state_carry
    query_block, key_block, value_block, input_block, forget_block = inputs
    length = query_block.shape[0]
    highest = lax.Precision.HIGHEST
    query_scale = query_block.shape[2] ** (-0.5)
    causal = jnp.tril(jnp.ones((length, length), dtype=bool))[:, :, None]
    cumulative = jnp.cumsum(forget_block, axis=0)
    logits = cumulative[:, None, :] - cumulative[None, :, :] + input_block[None, :, :]
    logits = jnp.where(causal, logits, -jnp.inf)
    carried = cumulative + running[None, :]
    stable = jnp.maximum(carried, jnp.max(logits, axis=1))
    carry_weight = jnp.exp(carried - stable)
    raw = (
        jnp.einsum("thd,shd->tsh", query_block, key_block, preferred_element_type=jnp.float32)
        * query_scale
    )
    scores = raw * jnp.exp(logits - stable[:, None, :])
    scaled_query = query_block.astype(jnp.float32) * query_scale
    numerator = carry_weight[:, :, None] * jnp.einsum(
        "hvd,thd->thv", memory, scaled_query, precision=highest
    )
    numerator = numerator + jnp.einsum(
        "tsh,shv->thv", scores.astype(jnp.bfloat16), value_block, preferred_element_type=jnp.float32
    )
    denominator = carry_weight * jnp.einsum(
        "hd,thd->th", normer, scaled_query, precision=highest
    ) + jnp.sum(scores, axis=1)
    last_sum = cumulative[-1]
    weights_log = last_sum[None, :] - cumulative + input_block
    new_running = jnp.maximum(last_sum + running, jnp.max(weights_log, axis=0))
    decay_factor = jnp.exp(last_sum + running - new_running)
    weighted = (
        key_block.astype(jnp.float32) * jnp.exp(weights_log - new_running[None, :])[:, :, None]
    )
    memory = decay_factor[:, None, None] * memory + jnp.einsum(
        "shv,shd->hvd",
        value_block,
        weighted.astype(jnp.bfloat16),
        preferred_element_type=jnp.float32,
    )
    normer = decay_factor[:, None] * normer + jnp.sum(weighted, axis=0)
    return ((memory, normer, new_running), (numerator, denominator, stable))


def local(
    residual_entry_input,
    query_matrix_rows,
    key_matrix_rows,
    value_matrix_rows,
    output_gate_logits,
    input_gate_logits,
    forget_gate_logits,
    forget_decay_offset,
    head_norm_gain,
    cell_output_weight,
    feedforward_norm_gain,
    gate_up_weight,
    value_up_weight,
    gate_filter_taps,
    value_filter_taps,
    down_projection_weight,
):
    highest = lax.Precision.HIGHEST
    token_count = query_matrix_rows.shape[0]
    head_count = input_gate_logits.shape[1]
    key_width = query_matrix_rows.shape[1] // head_count
    value_width = value_matrix_rows.shape[1] // head_count
    query_scale = key_width ** (-0.5)
    queries_low = query_matrix_rows.reshape(token_count, head_count, key_width)
    keys_low = key_matrix_rows.reshape(token_count, head_count, key_width)
    values_low = value_matrix_rows.reshape(token_count, head_count, value_width)
    input_log_value, forget_log_sigmoid = gate_log_values(
        input_gate_logits, forget_gate_logits, forget_decay_offset
    )
    cumulative = jnp.cumsum(forget_log_sigmoid, axis=0)
    total_log = cumulative[-1]
    block_count = token_count // BLOCK

    def blocks(tensor):
        return tensor.reshape((block_count, BLOCK) + tensor.shape[1:])

    initial = (
        jnp.zeros((head_count, value_width, key_width), jnp.float32),
        jnp.zeros((head_count, key_width), jnp.float32),
        jnp.full((head_count,), neg_large, jnp.float32),
    )
    end_state, (numerator, denominator, stable) = lax.scan(
        local_step,
        initial,
        (
            blocks(queries_low),
            blocks(keys_low),
            blocks(values_low),
            blocks(input_log_value),
            blocks(forget_log_sigmoid),
        ),
    )
    end_memory, end_normer, end_running = end_state
    identity = (
        jnp.zeros((head_count,), jnp.float32),
        jnp.zeros((head_count, value_width, key_width), jnp.float32),
        jnp.zeros((head_count, key_width), jnp.float32),
        jnp.full((head_count,), neg_large, jnp.float32),
    )
    prefix = carried_in(
        (total_log, end_memory, end_normer, end_running), "sp", combine_states, identity
    )
    numerator = numerator.reshape(token_count, head_count, value_width)
    denominator = denominator.reshape(token_count, head_count)
    stable = stable.reshape(token_count, head_count)
    _, prior_memory, prior_normer, prior_running = prefix
    scaled_query = queries_low.astype(jnp.float32) * query_scale
    prior_log = cumulative + prior_running[None, :]
    top_log = jnp.maximum(stable, prior_log)
    local_weight = jnp.exp(stable - top_log)
    prior_weight = jnp.exp(prior_log - top_log)
    numerator = local_weight[:, :, None] * numerator + prior_weight[:, :, None] * jnp.einsum(
        "hvd,thd->thv", prior_memory, scaled_query, precision=highest
    )
    denominator = local_weight * denominator + prior_weight * jnp.einsum(
        "hd,thd->th", prior_normer, scaled_query, precision=highest
    )
    memory_out = numerator / jnp.maximum(jnp.abs(denominator), jnp.exp(-top_log))[:, :, None]
    normed = (
        memory_out
        * lax.rsqrt(jnp.mean(memory_out * memory_out, axis=-1, keepdims=True) + eps)
        * head_norm_gain[None, :, :]
    )
    gated_rows = (
        normed.reshape(token_count, head_count * value_width)
        * jax.nn.sigmoid(output_gate_logits.astype(jnp.float32))
    ).astype(jnp.bfloat16)
    whole_out = lax.all_gather(cell_output_weight, "tp", axis=0, tiled=True)
    own_rows = lax.all_to_all(gated_rows, "tp", split_axis=0, concat_axis=1, tiled=True)
    mixed_rows = jnp.dot(own_rows, whole_out, preferred_element_type=jnp.float32)
    stream_wide = residual_entry_input.astype(jnp.float32) + mixed_rows
    stream = stream_wide.astype(jnp.bfloat16)
    stream_wide = lax.optimization_barrier(stream).astype(jnp.float32)
    normed_rows = (
        stream_wide
        * lax.rsqrt(jnp.mean(stream_wide * stream_wide, axis=-1, keepdims=True) + eps)
        * feedforward_norm_gain[None, :]
    ).astype(jnp.bfloat16)
    group_rows = lax.all_gather(normed_rows, "tp", axis=0, tiled=True)
    earlier_rows = shifted(group_rows[-2:], "sp", 1)
    window = jnp.concatenate([earlier_rows, group_rows], axis=0)
    up_gate = jnp.dot(
        window,
        lax.all_gather(gate_up_weight, "sp", axis=0, tiled=True),
        preferred_element_type=jnp.float32,
    )
    up_value = jnp.dot(
        window,
        lax.all_gather(value_up_weight, "sp", axis=0, tiled=True),
        preferred_element_type=jnp.float32,
    )
    conv_g = (
        gate_filter_taps[0][None, :] * up_gate[:-2]
        + gate_filter_taps[1][None, :] * up_gate[1:-1]
        + gate_filter_taps[2][None, :] * up_gate[2:]
    )
    conv_v = (
        value_filter_taps[0][None, :] * up_value[:-2]
        + value_filter_taps[1][None, :] * up_value[1:-1]
        + value_filter_taps[2][None, :] * up_value[2:]
    )
    hidden = (jax.nn.silu(conv_g) * conv_v).astype(jnp.bfloat16)
    whole_down = lax.all_gather(down_projection_weight, "sp", axis=1, tiled=True)
    ffn_rows = lax.psum_scatter(
        jnp.dot(hidden, whole_down, preferred_element_type=jnp.float32).astype(jnp.bfloat16),
        "tp",
        scatter_dimension=0,
        tiled=True,
    ).astype(jnp.float32)
    return (stream_wide + ffn_rows).astype(jnp.bfloat16)


def solution(mesh):
    in_specs = (
        P(("sp", "tp"), None),
        P("sp", "tp"),
        P("sp", "tp"),
        P("sp", "tp"),
        P("sp", "tp"),
        P("sp", "tp"),
        P("sp", "tp"),
        P("sp", "tp"),
        P("tp", None),
        P("tp", None),
        P(),
        P("sp", "tp"),
        P("sp", "tp"),
        P(None, "tp"),
        P(None, "tp"),
        P("tp", "sp"),
    )
    out_specs = P(("sp", "tp"), None)
    return jax.shard_map(local, mesh=mesh, in_specs=in_specs, out_specs=out_specs, check_vma=False)
```

profile of v0, /device:TPU:0, one launch (start us, length us, event | category | flops | bytes accessed | tf_op | source)
XLA Modules:
  0.0 629.0 jit_solution(18224603662122398015)
XLA Ops:
  12.8 105.2 %while.39 = (s32[]{:T(128)}, f32[2,256,128]{2,1,0:T(8,128)S(1)}, f32[2,128]{1,0:T(2,128)S(1)}, f32[2]{0:T(128)S(1)}, f32[8,128,2,256]{1,0,3,2:T(8,128)}, /*index...) while((s32[]{:T(128)}, f32[2,256,128]{2,1,0:T(8,128)S(1)}, ...), condition=%wide.region_6.7_spmd.clone, body=%wide.region_0.6_spmd.clone.sunk | while | flops 144166400 | bytes 4685610 | solution.py:144
  17.3 8.2 %dynamic_update_slice.19 = f32[8,128,2,256]{1,0,3,2:T(8,128)} dynamic-update-slice(f32[8,128,2,256]{1,0,3,2:T(8,128)} %get-tuple-element.661, f32[1,128,2,256]{1,0,3,2:T(1,128)S(1)} %copy.248, s32[]{:T(128)} %get-tuple-element.657, s32[]{:T(128)} %constant.83.clone.1..sunk, s32[]{:T(128)} %constant.83.clone.1..sunk, s32[]{:T(128)} %constant.83.clone.1..sunk) | dynamic-update-slice | bytes 524292 | tf_op jit(solution)/shard_map/while/body/jit(dynamic_update_index_in_dim)/dynamic_update_slice | solution.py:144
  30.5 8.2 %dynamic_update_slice.19 = f32[8,128,2,256]{1,0,3,2:T(8,128)} dynamic-update-slice(f32[8,128,2,256]{1,0,3,2:T(8,128)} %get-tuple-element.661, f32[1,128,2,256]{1,0,3,2:T(1,128)S(1)} %copy.248, s32[]{:T(128)} %get-tuple-element.657, s32[]{:T(128)} %constant.83.clone.1..sunk, s32[]{:T(128)} %constant.83.clone.1..sunk, s32[]{:T(128)} %constant.83.clone.1..sunk) | dynamic-update-slice | bytes 524292 | tf_op jit(solution)/shard_map/while/body/jit(dynamic_update_index_in_dim)/dynamic_update_slice | solution.py:144
  43.7 8.2 %dynamic_update_slice.19 = f32[8,128,2,256]{1,0,3,2:T(8,128)} dynamic-update-slice(f32[8,128,2,256]{1,0,3,2:T(8,128)} %get-tuple-element.661, f32[1,128,2,256]{1,0,3,2:T(1,128)S(1)} %copy.248, s32[]{:T(128)} %get-tuple-element.657, s32[]{:T(128)} %constant.83.clone.1..sunk, s32[]{:T(128)} %constant.83.clone.1..sunk, s32[]{:T(128)} %constant.83.clone.1..sunk) | dynamic-update-slice | bytes 524292 | tf_op jit(solution)/shard_map/while/body/jit(dynamic_update_index_in_dim)/dynamic_update_slice | solution.py:144
  56.8 8.2 %dynamic_update_slice.19 = f32[8,128,2,256]{1,0,3,2:T(8,128)} dynamic-update-slice(f32[8,128,2,256]{1,0,3,2:T(8,128)} %get-tuple-element.661, f32[1,128,2,256]{1,0,3,2:T(1,128)S(1)} %copy.248, s32[]{:T(128)} %get-tuple-element.657, s32[]{:T(128)} %constant.83.clone.1..sunk, s32[]{:T(128)} %constant.83.clone.1..sunk, s32[]{:T(128)} %constant.83.clone.1..sunk) | dynamic-update-slice | bytes 524292 | tf_op jit(solution)/shard_map/while/body/jit(dynamic_update_index_in_dim)/dynamic_update_slice | solution.py:144
  70.0 8.2 %dynamic_update_slice.19 = f32[8,128,2,256]{1,0,3,2:T(8,128)} dynamic-update-slice(f32[8,128,2,256]{1,0,3,2:T(8,128)} %get-tuple-element.661, f32[1,128,2,256]{1,0,3,2:T(1,128)S(1)} %copy.248, s32[]{:T(128)} %get-tuple-element.657, s32[]{:T(128)} %constant.83.clone.1..sunk, s32[]{:T(128)} %constant.83.clone.1..sunk, s32[]{:T(128)} %constant.83.clone.1..sunk) | dynamic-update-slice | bytes 524292 | tf_op jit(solution)/shard_map/while/body/jit(dynamic_update_index_in_dim)/dynamic_update_slice | solution.py:144
  83.1 8.2 %dynamic_update_slice.19 = f32[8,128,2,256]{1,0,3,2:T(8,128)} dynamic-update-slice(f32[8,128,2,256]{1,0,3,2:T(8,128)} %get-tuple-element.661, f32[1,128,2,256]{1,0,3,2:T(1,128)S(1)} %copy.248, s32[]{:T(128)} %get-tuple-element.657, s32[]{:T(128)} %constant.83.clone.1..sunk, s32[]{:T(128)} %constant.83.clone.1..sunk, s32[]{:T(128)} %constant.83.clone.1..sunk) | dynamic-update-slice | bytes 524292 | tf_op jit(solution)/shard_map/while/body/jit(dynamic_update_index_in_dim)/dynamic_update_slice | solution.py:144
  96.3 8.2 %dynamic_update_slice.19 = f32[8,128,2,256]{1,0,3,2:T(8,128)} dynamic-update-slice(f32[8,128,2,256]{1,0,3,2:T(8,128)} %get-tuple-element.661, f32[1,128,2,256]{1,0,3,2:T(1,128)S(1)} %copy.248, s32[]{:T(128)} %get-tuple-element.657, s32[]{:T(128)} %constant.83.clone.1..sunk, s32[]{:T(128)} %constant.83.clone.1..sunk, s32[]{:T(128)} %constant.83.clone.1..sunk) | dynamic-update-slice | bytes 524292 | tf_op jit(solution)/shard_map/while/body/jit(dynamic_update_index_in_dim)/dynamic_update_slice | solution.py:144
  109.4 8.2 %dynamic_update_slice.19 = f32[8,128,2,256]{1,0,3,2:T(8,128)} dynamic-update-slice(f32[8,128,2,256]{1,0,3,2:T(8,128)} %get-tuple-element.661, f32[1,128,2,256]{1,0,3,2:T(1,128)S(1)} %copy.248, s32[]{:T(128)} %get-tuple-element.657, s32[]{:T(128)} %constant.83.clone.1..sunk, s32[]{:T(128)} %constant.83.clone.1..sunk, s32[]{:T(128)} %constant.83.clone.1..sunk) | dynamic-update-slice | bytes 524292 | tf_op jit(solution)/shard_map/while/body/jit(dynamic_update_index_in_dim)/dynamic_update_slice | solution.py:144
  122.2 22.3 %all-gather.3 = bf16[8,1,2]{2,1,0:T(2,128)(2,1)S(1)} all-gather(bf16[1,1,2]{2,1,0:T(2,128)(2,1)S(1)} %bitcast.273), channel_id=1, replica_groups=mesh['sp'=8,'tp'=4] {'sp'}, dimensions={0}, use_global_device_ids=true | all-gather | bytes 36 | tf_op jit(solution)/shard_map/all_gather | solution.py:14
  144.5 17.5 %all-reduce = bf16[16]{0:T(256)(128)(2,1)S(1)} all-reduce(bf16[16]{0:T(256)(128)(2,1)S(1)} %dynamic-update-slice), channel_id=2, replica_groups=mesh['sp'=8,'tp'=4] {'sp'}, use_global_device_ids=true, to_apply=%add | all-reduce | flops 16 | bytes 64
  166.5 18.0 %all-gather.4 = bf16[8,2,128]{2,1,0:T(2,128)(2,1)S(1)} all-gather(bf16[1,2,128]{2,1,0:T(2,128)(2,1)S(1)} %convert_bitcast_fusion), channel_id=4, replica_groups=mesh['sp'=8,'tp'=4] {'sp'}, dimensions={0}, use_global_device_ids=true | all-gather | bytes 4608 | tf_op jit(solution)/shard_map/all_gather | solution.py:14
  184.5 10.5 %while.40 = (s32[]{:T(128)}, f32[2,256,128]{2,1,0:T(8,128)S(1)}, f32[2,128]{1,0:T(2,128)S(1)}, f32[2]{0:T(128)S(1)}, s32[]{:T(128)}, /*index=5*/bf16[8,2]{0,1:T(...) while((s32[]{:T(128)}, f32[2,256,128]{2,1,0:T(8,128)S(1)}, ...), condition=%wide.region_10.11_spmd.clone, body=%wide.region_9.10_spmd.clone.sunk | while | flops 394772 | bytes 658157 | solution.py:29
  203.1 26.9 %all_to_all.19 = bf16[4,256,512]{2,1,0:T(8,128)(2,1)S(1)} all-to-all(bf16[4,256,512]{2,1,0:T(8,128)(2,1)S(1)} %bitcast.262), channel_id=1, replica_groups=mesh['sp'=8,'tp'=4] {'tp'}, dimensions={0} | all-to-all | bytes 2097152 | tf_op jit(solution)/shard_map/all_to_all | solution.py:191
  230.5 5.7 fusion.45
  239.9 33.9 %all-gather.14.cloned.1.call-done = bf16[1024,2048]{1,0:T(8,128)(2,1)} async-done(((bf16[256,2048]{1,0:T(8,128)(2,1)}), bf16[1024,2048]{1,0:T(8,128)(2,1)}) %all-gather.14.cloned.1.call-update) | async-done | bytes 4194320 | tf_op jit(solution)/shard_map/all_gather | solution.py:201
  274.6 3.4 collective-permute-start
  278.1 90.1 %all-gather.16.cloned.1.call-done = bf16[2048,1408]{1,0:T(8,128)(2,1)} async-done(((bf16[256,1408]{1,0:T(8,128)(2,1)}), bf16[2048,1408]{1,0:T(8,128)(2,1)}) %all-gather.16.cloned.1.call-update) | async-done | bytes 5767184 | tf_op jit(solution)/shard_map/all_gather | solution.py:206
  368.2 11.9 %fusion.44 = f32[1026,1408]{1,0:T(8,128)} fusion(bf16[2048,1408]{1,0:T(8,128)(2,1)} %all-gather.16.cloned.1.call-done, bf16[1024,2048]{1,0:T(8,128)(2,1)} %all-gather.14.cloned.1.call-done, bf16[2,2048]{1,0:T(2,128)(2,1)S(1)} %collective-permute-done), kind=kOutput, calls=%fused_computation.90 | convolution fusion | flops 5925519360 | bytes 15748096 | tf_op jit(solution)/shard_map/dot_general | solution.py:204
  380.1 80.6 %all-gather.18.cloned.1.call-done = bf16[2048,1408]{1,0:T(8,128)(2,1)} async-done(((bf16[256,1408]{1,0:T(8,128)(2,1)}), bf16[2048,1408]{1,0:T(8,128)(2,1)}) %all-gather.18.cloned.1.call-update) | async-done | bytes 5767184 | tf_op jit(solution)/shard_map/all_gather | solution.py:211
  460.7 11.9 %fusion.43 = f32[1026,1408]{1,0:T(8,128)} fusion(bf16[2048,1408]{1,0:T(8,128)(2,1)} %all-gather.18.cloned.1.call-done, bf16[1024,2048]{1,0:T(8,128)(2,1)} %all-gather.14.cloned.1.call-done, bf16[2,2048]{1,0:T(2,128)(2,1)S(1)} %collective-permute-done), kind=kOutput, calls=%fused_computation.89 | convolution fusion | flops 5925519360 | bytes 15748096 | tf_op jit(solution)/shard_map/dot_general | solution.py:209
  472.6 81.3 %all-gather.20.cloned.1.call-done = bf16[1408,2048]{1,0:T(8,128)(2,1)} async-done(((bf16[1408,256]{1,0:T(8,128)(2,1)}), bf16[1408,2048]{1,0:T(8,128)(2,1)}) %all-gather.20.cloned.1.call-update) | async-done | bytes 5767184 | tf_op jit(solution)/shard_map/all_gather | solution.py:225
  554.0 22.7 %convolution_convert_fusion = bf16[1024,2048]{1,0:T(8,128)(2,1)} fusion(bf16[1408,2048]{1,0:T(8,128)(2,1)} %all-gather.20.cloned.1.call-done, f32[1026,1408]{1,0:T(8,128)} %fusion.43, f32[1026,1408]{1,0:T(8,128)} %fusion.44, f32[1408]{0:T(1024)S(1)} %get-tuple-element.403, f32[1408]{0:T(1024)S(1)} %get-tuple-element.404, f32[1408]{0:T(1024)S(1)} %get-tuple-element.402, ...), kind=kOutput, calls=%fused_computation.85 | convolution fusion | flops 5930745856 | bytes 44598272 | tf_op jit(solution)/shard_map/dot_general | solution.py:227
  576.7 42.9 %reduce-scatter.2.cloned.1.call-done = bf16[256,2048]{1,0:T(8,128)(2,1)} async-done(((bf16[1024,2048]{1,0:T(8,128)(2,1)}), bf16[256,2048]{1,0:T(8,128)(2,1)}) %reduce-scatter.2.cloned.1.call-update) | async-done | bytes 1048592 | tf_op jit(solution)/shard_map/reduce_scatter | solution.py:226
  (345 shorter events, 78.8 us)
Async XLA Ops:
  6.5 5.3 copy-start.1
  6.5 178.0 %all-gather.22.cloned.1.call-start = ((), (), s32[]{:S(2)}) async-start(), calls=%async_computation.8 | async-start | bytes 1179648 | tf_op jit(solution)/shard_map/all_gather | solution.py:14
  12.8 107.7 %copy-start.7 = (u32[32]{0:T(128)S(1)}, u32[32]{0:T(128)}, u32[]{:S(2)}) copy-start(u32[32]{0:T(128)} %constant.101) | copy-start | bytes 388
  118.7 111.8 %all-gather.12.cloned.1.call-start = ((), (), s32[]{:S(2)}) async-start(), calls=%async_computation.2 | async-start | bytes 10485760 | tf_op jit(solution)/shard_map/all_gather | solution.py:190
  119.4 154.4 %all-gather.14.cloned.1.call-start = ((), (), s32[]{:S(2)}) async-start(), calls=%async_computation.3 | async-start | bytes 5242880 | tf_op jit(solution)/shard_map/all_gather | solution.py:201
  163.5 31.6 %copy-start.2 = (bf16[1024,256]{1,0:T(8,128)(2,1)S(1)}, bf16[1024,256]{1,0:T(8,128)(2,1)}, u32[]{:S(2)}) copy-start(bf16[1024,256]{1,0:T(8,128)(2,1)} %param.21) | copy-start | bytes 1572868
  196.2 2.3 copy-start.6
  200.6 29.9 %copy-start = (bf16[256,2048]{1,0:T(8,128)(2,1)S(1)}, bf16[256,2048]{1,0:T(8,128)(2,1)}, u32[]{:S(2)}) copy-start(bf16[256,2048]{1,0:T(8,128)(2,1)} %param.20) | copy-start | bytes 3145732
  230.5 6.1 copy-start.5
  236.3 41.7 %copy-start.3 = (f32[3,1408]{1,0:T(4,128)S(1)}, f32[3,1408]{1,0:T(4,128)}, u32[]{:S(2)}) copy-start(f32[3,1408]{1,0:T(4,128)} %param.34) | copy-start | bytes 50692
  236.3 41.7 %copy-start.4 = (f32[3,1408]{1,0:T(4,128)S(1)}, f32[3,1408]{1,0:T(4,128)}, u32[]{:S(2)}) copy-start(f32[3,1408]{1,0:T(4,128)} %param.33) | copy-start | bytes 50692
  237.9 130.3 %all-gather.16.cloned.1.call-start = ((), (), s32[]{:S(2)}) async-start(), calls=%async_computation.4 | async-start | bytes 6488064 | tf_op jit(solution)/shard_map/all_gather | solution.py:206
  238.5 222.3 %all-gather.18.cloned.1.call-start = ((), (), s32[]{:S(2)}) async-start(), calls=%async_computation.5 | async-start | bytes 6488064 | tf_op jit(solution)/shard_map/all_gather | solution.py:211
  239.1 314.9 %all-gather.20.cloned.1.call-start = ((), (), s32[]{:S(2)}) async-start(), calls=%async_computation.6 | async-start | bytes 6488064 | tf_op jit(solution)/shard_map/all_gather | solution.py:225
  239.7 379.9 %reduce-scatter.2.cloned.1.call-start = ((), (), s32[]{:S(2)}) async-start(), calls=%async_computation.7 | async-start | bytes 5242880 | tf_op jit(solution)/shard_map/reduce_scatter | solution.py:226
  274.6 93.6 %collective-permute-start = (bf16[2,2048]{1,0:T(2,128)(2,1)S(1)}, bf16[2,2048]{1,0:T(2,128)(2,1)S(1)}, u32[]{:S(2)}, u32[]{:S(2)}) collective-permute-start(bf16[2,2048]{1,0:T(2,128)(2,1)S(1)} %slice.72), channel_id=1, source_target_pairs={{0,4},{4,8},{8,12},{12,16},{16,20},{20,24},{24,28},{1,5},{5,9},{9,... | collective-permute-start | bytes 24584 | tf_op jit(solution)/shard_map/ppermute | solution.py:35
Sparse Core Ops, SparseCore 0:
  118.8 43.2 all-gather.21
  163.6 66.6 all-gather.11
  238.0 35.7 all-gather.13
  275.8 92.3 all-gather.15
  370.2 90.4 all-gather.17
  462.6 91.2 all-gather.19
  576.8 42.7 reduce-scatter.1
where the time goes:
time: 631 us; the launch traced here: 629 us
  waiting for transfers between devices  331 us (52%)
  local copies, waits for them, and re-layouts  97.1 us (15%)
  blocking collectives  84.7 us (13%)
  matrix products  67.5 us (11%)
  other arithmetic  29.4 us (5%)
  between operations  14.4 us (2%)
    all_gather x1, waiting for transfers between devices, local(): lax.all_gather(gate_up_weight, 'sp', axis=0, tiled=True)  90.1 us
    all_gather x1, waiting for transfers between devices, local(): lax.all_gather(down_projection_weight, 'sp', axis=1, tiled=True)  81.3 us
    all_gather x1, waiting for transfers between devices, local(): lax.all_gather(value_up_weight, 'sp', axis=0, tiled=True)  80.6 us
    dynamic_update_slice x16, local copies, waits for them, and re-layouts, local(): lax.scan(local_step, initial, (blocks(queries_low), blocks(keys_low), blo...  66.7 us
    reduce_scatter x1, waiting for transfers between devices, local(): lax.psum_scatter(jnp.dot(hidden, whole_down, preferred_element_type=jnp.f...  42.9 us
    all_gather x2, blocking collectives, carried_in(): lax.all_gather(part.astype(kind), axis)  40.3 us
    all_gather x1, waiting for transfers between devices, local(): group_rows = lax.all_gather(normed_rows, 'tp', axis=0, tiled=True)  33.9 us
    all_to_all x1, blocking collectives, local(): lax.all_to_all(gated_rows, 'tp', split_axis=0, concat_axis=1, tiled=True)  26.9 us
  transfers between devices with their start and end apart: 8, of which 5 were waited for; matrix products, arithmetic and copies ran while one was open for 8% of the time, Pallas kernels for 0%

commit v1 on v0

--- a/solution.py
+++ b/solution.py
@@ -198,7 +198,10 @@
         * lax.rsqrt(jnp.mean(stream_wide * stream_wide, axis=-1, keepdims=True) + eps)
         * feedforward_norm_gain[None, :]
     ).astype(jnp.bfloat16)
-    group_rows = lax.all_gather(normed_rows, "tp", axis=0, tiled=True)
+    size = lax.axis_size("tp")
+    parts = jnp.stack([normed_rows for _ in range(size)])
+    parts = lax.all_to_all(parts, "tp", split_axis=0, concat_axis=0)
+    group_rows = jnp.concatenate(parts, axis=0)
     earlier_rows = shifted(group_rows[-2:], "sp", 1)
     window = jnp.concatenate([earlier_rows, group_rows], axis=0)
     up_gate = jnp.dot(

time: 631 us -> 590 us (0.935)
  waiting for transfers between devices: 331 us -> 239 us
  blocking collectives: 84.7 us -> 136 us
    all_gather x1, waiting for transfers between devices: 90.1 us -> 31.5 us  [local(): lax.all_gather(gate_up_weight, 'sp', axis=0, tiled=True)]
    all_to_all x0 -> x1, blocking collectives: none -> 50.8 us  [local(): parts = lax.all_to_all(parts, 'tp', split_axis=0, concat_axis=0)]
    all_gather x1 -> x0, waiting for transfers between devices: 33.9 us -> none  [local(): group_rows = lax.all_gather(normed_rows, 'tp', axis=0, tiled=True)]
  transfers between devices with their start and end apart: 8 -> 7, of which waited for: 5 -> 4; matrix products, arithmetic and copies ran while one was open for 8% -> 9% of each run, Pallas kernels for 0% -> 0%
where the time goes in v1:
time: 590 us; the launch traced here: 587 us
  waiting for transfers between devices  239 us (41%)
  blocking collectives  136 us (23%)
  local copies, waits for them, and re-layouts  96.7 us (16%)
  matrix products  67.4 us (11%)
  other arithmetic  28.4 us (5%)
  between operations  14.4 us (2%)
    all_gather x1, waiting for transfers between devices, local(): lax.all_gather(down_projection_weight, 'sp', axis=1, tiled=True)  81.3 us
    all_gather x1, waiting for transfers between devices, local(): lax.all_gather(value_up_weight, 'sp', axis=0, tiled=True)  80.7 us
    dynamic_update_slice x16, local copies, waits for them, and re-layouts, local(): lax.scan(local_step, initial, (blocks(queries_low), blocks(keys_low), blo...  66.7 us
    all_to_all x1, blocking collectives, local(): parts = lax.all_to_all(parts, 'tp', split_axis=0, concat_axis=0)  50.8 us
    reduce_scatter x1, waiting for transfers between devices, local(): lax.psum_scatter(jnp.dot(hidden, whole_down, preferred_element_type=jnp.f...  42.9 us
    all_gather x2, blocking collectives, carried_in(): lax.all_gather(part.astype(kind), axis)  34.7 us
    all_gather x1, waiting for transfers between devices, local(): lax.all_gather(gate_up_weight, 'sp', axis=0, tiled=True)  31.5 us
    all_to_all x1, blocking collectives, local(): lax.all_to_all(gated_rows, 'tp', split_axis=0, concat_axis=1, tiled=True)  26.9 us
  transfers between devices with their start and end apart: 7, of which 4 were waited for; matrix products, arithmetic and copies ran while one was open for 9% of the time, Pallas kernels for 0%

profile of v1, /device:TPU:0, one launch (start us, length us, event | category | flops | bytes accessed | tf_op | source)
XLA Modules:
  0.0 587.2 jit_solution(6658395831791031615)
XLA Ops:
  12.8 105.2 %while.39 = (s32[]{:T(128)}, f32[2,256,128]{2,1,0:T(8,128)S(1)}, f32[2,128]{1,0:T(2,128)S(1)}, f32[2]{0:T(128)S(1)}, f32[8,128,2,256]{1,0,3,2:T(8,128)}, /*index...) while((s32[]{:T(128)}, f32[2,256,128]{2,1,0:T(8,128)S(1)}, ...), condition=%wide.region_6.7_spmd.clone, body=%wide.region_0.6_spmd.clone.sunk | while | flops 144166400 | bytes 4685610 | solution.py:144
  17.3 8.2 %dynamic_update_slice.19 = f32[8,128,2,256]{1,0,3,2:T(8,128)} dynamic-update-slice(f32[8,128,2,256]{1,0,3,2:T(8,128)} %get-tuple-element.661, f32[1,128,2,256]{1,0,3,2:T(1,128)S(1)} %copy.248, s32[]{:T(128)} %get-tuple-element.657, s32[]{:T(128)} %constant.83.clone.1..sunk, s32[]{:T(128)} %constant.83.clone.1..sunk, s32[]{:T(128)} %constant.83.clone.1..sunk) | dynamic-update-slice | bytes 524292 | tf_op jit(solution)/shard_map/while/body/jit(dynamic_update_index_in_dim)/dynamic_update_slice | solution.py:144
  30.5 8.2 %dynamic_update_slice.19 = f32[8,128,2,256]{1,0,3,2:T(8,128)} dynamic-update-slice(f32[8,128,2,256]{1,0,3,2:T(8,128)} %get-tuple-element.661, f32[1,128,2,256]{1,0,3,2:T(1,128)S(1)} %copy.248, s32[]{:T(128)} %get-tuple-element.657, s32[]{:T(128)} %constant.83.clone.1..sunk, s32[]{:T(128)} %constant.83.clone.1..sunk, s32[]{:T(128)} %constant.83.clone.1..sunk) | dynamic-update-slice | bytes 524292 | tf_op jit(solution)/shard_map/while/body/jit(dynamic_update_index_in_dim)/dynamic_update_slice | solution.py:144
  43.6 8.2 %dynamic_update_slice.19 = f32[8,128,2,256]{1,0,3,2:T(8,128)} dynamic-update-slice(f32[8,128,2,256]{1,0,3,2:T(8,128)} %get-tuple-element.661, f32[1,128,2,256]{1,0,3,2:T(1,128)S(1)} %copy.248, s32[]{:T(128)} %get-tuple-element.657, s32[]{:T(128)} %constant.83.clone.1..sunk, s32[]{:T(128)} %constant.83.clone.1..sunk, s32[]{:T(128)} %constant.83.clone.1..sunk) | dynamic-update-slice | bytes 524292 | tf_op jit(solution)/shard_map/while/body/jit(dynamic_update_index_in_dim)/dynamic_update_slice | solution.py:144
  56.8 8.2 %dynamic_update_slice.19 = f32[8,128,2,256]{1,0,3,2:T(8,128)} dynamic-update-slice(f32[8,128,2,256]{1,0,3,2:T(8,128)} %get-tuple-element.661, f32[1,128,2,256]{1,0,3,2:T(1,128)S(1)} %copy.248, s32[]{:T(128)} %get-tuple-element.657, s32[]{:T(128)} %constant.83.clone.1..sunk, s32[]{:T(128)} %constant.83.clone.1..sunk, s32[]{:T(128)} %constant.83.clone.1..sunk) | dynamic-update-slice | bytes 524292 | tf_op jit(solution)/shard_map/while/body/jit(dynamic_update_index_in_dim)/dynamic_update_slice | solution.py:144
  70.0 8.2 %dynamic_update_slice.19 = f32[8,128,2,256]{1,0,3,2:T(8,128)} dynamic-update-slice(f32[8,128,2,256]{1,0,3,2:T(8,128)} %get-tuple-element.661, f32[1,128,2,256]{1,0,3,2:T(1,128)S(1)} %copy.248, s32[]{:T(128)} %get-tuple-element.657, s32[]{:T(128)} %constant.83.clone.1..sunk, s32[]{:T(128)} %constant.83.clone.1..sunk, s32[]{:T(128)} %constant.83.clone.1..sunk) | dynamic-update-slice | bytes 524292 | tf_op jit(solution)/shard_map/while/body/jit(dynamic_update_index_in_dim)/dynamic_update_slice | solution.py:144
  83.1 8.2 %dynamic_update_slice.19 = f32[8,128,2,256]{1,0,3,2:T(8,128)} dynamic-update-slice(f32[8,128,2,256]{1,0,3,2:T(8,128)} %get-tuple-element.661, f32[1,128,2,256]{1,0,3,2:T(1,128)S(1)} %copy.248, s32[]{:T(128)} %get-tuple-element.657, s32[]{:T(128)} %constant.83.clone.1..sunk, s32[]{:T(128)} %constant.83.clone.1..sunk, s32[]{:T(128)} %constant.83.clone.1..sunk) | dynamic-update-slice | bytes 524292 | tf_op jit(solution)/shard_map/while/body/jit(dynamic_update_index_in_dim)/dynamic_update_slice | solution.py:144
  96.3 8.2 %dynamic_update_slice.19 = f32[8,128,2,256]{1,0,3,2:T(8,128)} dynamic-update-slice(f32[8,128,2,256]{1,0,3,2:T(8,128)} %get-tuple-element.661, f32[1,128,2,256]{1,0,3,2:T(1,128)S(1)} %copy.248, s32[]{:T(128)} %get-tuple-element.657, s32[]{:T(128)} %constant.83.clone.1..sunk, s32[]{:T(128)} %constant.83.clone.1..sunk, s32[]{:T(128)} %constant.83.clone.1..sunk) | dynamic-update-slice | bytes 524292 | tf_op jit(solution)/shard_map/while/body/jit(dynamic_update_index_in_dim)/dynamic_update_slice | solution.py:144
  109.4 8.2 %dynamic_update_slice.19 = f32[8,128,2,256]{1,0,3,2:T(8,128)} dynamic-update-slice(f32[8,128,2,256]{1,0,3,2:T(8,128)} %get-tuple-element.661, f32[1,128,2,256]{1,0,3,2:T(1,128)S(1)} %copy.248, s32[]{:T(128)} %get-tuple-element.657, s32[]{:T(128)} %constant.83.clone.1..sunk, s32[]{:T(128)} %constant.83.clone.1..sunk, s32[]{:T(128)} %constant.83.clone.1..sunk) | dynamic-update-slice | bytes 524292 | tf_op jit(solution)/shard_map/while/body/jit(dynamic_update_index_in_dim)/dynamic_update_slice | solution.py:144
  123.0 23.3 %all-reduce = bf16[16]{0:T(256)(128)(2,1)S(1)} all-reduce(bf16[16]{0:T(256)(128)(2,1)S(1)} %dynamic-update-slice), channel_id=2, replica_groups=mesh['sp'=8,'tp'=4] {'sp'}, use_global_device_ids=true, to_apply=%add | all-reduce | flops 16 | bytes 64
  146.3 16.4 %all-gather.4 = bf16[8,2,128]{2,1,0:T(2,128)(2,1)S(1)} all-gather(bf16[1,2,128]{2,1,0:T(2,128)(2,1)S(1)} %convert_bitcast_fusion), channel_id=4, replica_groups=mesh['sp'=8,'tp'=4] {'sp'}, dimensions={0}, use_global_device_ids=true | all-gather | bytes 4608 | tf_op jit(solution)/shard_map/all_gather | solution.py:14
  163.9 18.3 %all-gather.3 = bf16[8,1,2]{2,1,0:T(2,128)(2,1)S(1)} all-gather(bf16[1,1,2]{2,1,0:T(2,128)(2,1)S(1)} %bitcast.279), channel_id=1, replica_groups=mesh['sp'=8,'tp'=4] {'sp'}, dimensions={0}, use_global_device_ids=true | all-gather | bytes 36 | tf_op jit(solution)/shard_map/all_gather | solution.py:14
  184.4 10.5 %while.40 = (s32[]{:T(128)}, f32[2,256,128]{2,1,0:T(8,128)S(1)}, f32[2,128]{1,0:T(2,128)S(1)}, f32[2]{0:T(128)S(1)}, s32[]{:T(128)}, /*index=5*/bf16[8,2]{0,1:T(...) while((s32[]{:T(128)}, f32[2,256,128]{2,1,0:T(8,128)S(1)}, ...), condition=%wide.region_10.11_spmd.clone, body=%wide.region_9.10_spmd.clone.sunk | while | flops 394772 | bytes 658157 | solution.py:29
  203.0 26.9 %all_to_all.24 = bf16[4,256,512]{2,1,0:T(8,128)(2,1)S(1)} all-to-all(bf16[4,256,512]{2,1,0:T(8,128)(2,1)S(1)} %bitcast.266), channel_id=1, replica_groups=mesh['sp'=8,'tp'=4] {'tp'}, dimensions={0} | all-to-all | bytes 2097152 | tf_op jit(solution)/shard_map/all_to_all | solution.py:191
  230.5 5.7 fusion.45
  237.4 50.8 %all_to_all.25 = bf16[4,256,2048]{2,1,0:T(8,128)(2,1)S(1)} all-to-all(bf16[4,256,2048]{2,1,0:T(8,128)(2,1)S(1)} %stack.2), channel_id=1, replica_groups=mesh['sp'=8,'tp'=4] {'tp'}, dimensions={0} | all-to-all | bytes 8388608 | tf_op jit(solution)/shard_map/all_to_all | solution.py:203
  290.2 4.6 collective-permute-start
  294.9 31.5 %all-gather.13.cloned.1.call-done = bf16[2048,1408]{1,0:T(8,128)(2,1)} async-done(((bf16[256,1408]{1,0:T(8,128)(2,1)}), bf16[2048,1408]{1,0:T(8,128)(2,1)}) %all-gather.13.cloned.1.call-update) | async-done | bytes 5767184 | tf_op jit(solution)/shard_map/all_gather | solution.py:209
  326.4 11.9 %fusion.44 = f32[1026,1408]{1,0:T(8,128)} fusion(bf16[2048,1408]{1,0:T(8,128)(2,1)} %all-gather.13.cloned.1.call-done, bf16[1024,2048]{1,0:T(8,128)(2,1)} %bitcast.263, bf16[2,2048]{1,0:T(2,128)(2,1)S(1)} %collective-permute-done), kind=kOutput, calls=%fused_computation.90 | convolution fusion | flops 5925519360 | bytes 15748096 | tf_op jit(solution)/shard_map/dot_general | solution.py:207
  338.3 80.7 %all-gather.15.cloned.1.call-done = bf16[2048,1408]{1,0:T(8,128)(2,1)} async-done(((bf16[256,1408]{1,0:T(8,128)(2,1)}), bf16[2048,1408]{1,0:T(8,128)(2,1)}) %all-gather.15.cloned.1.call-update) | async-done | bytes 5767184 | tf_op jit(solution)/shard_map/all_gather | solution.py:214
  419.0 11.9 %fusion.43 = f32[1026,1408]{1,0:T(8,128)} fusion(bf16[2048,1408]{1,0:T(8,128)(2,1)} %all-gather.15.cloned.1.call-done, bf16[1024,2048]{1,0:T(8,128)(2,1)} %bitcast.264, bf16[2,2048]{1,0:T(2,128)(2,1)S(1)} %collective-permute-done), kind=kOutput, calls=%fused_computation.89 | convolution fusion | flops 5925519360 | bytes 15748096 | tf_op jit(solution)/shard_map/dot_general | solution.py:212
  430.9 81.3 %all-gather.17.cloned.1.call-done = bf16[1408,2048]{1,0:T(8,128)(2,1)} async-done(((bf16[1408,256]{1,0:T(8,128)(2,1)}), bf16[1408,2048]{1,0:T(8,128)(2,1)}) %all-gather.17.cloned.1.call-update) | async-done | bytes 5767184 | tf_op jit(solution)/shard_map/all_gather | solution.py:228
  512.2 22.7 %convolution_convert_fusion = bf16[1024,2048]{1,0:T(8,128)(2,1)} fusion(bf16[1408,2048]{1,0:T(8,128)(2,1)} %all-gather.17.cloned.1.call-done, f32[1026,1408]{1,0:T(8,128)} %fusion.43, f32[1026,1408]{1,0:T(8,128)} %fusion.44, f32[1408]{0:T(1024)S(1)} %get-tuple-element.403, f32[1408]{0:T(1024)S(1)} %get-tuple-element.404, f32[1408]{0:T(1024)S(1)} %get-tuple-element.402, ...), kind=kOutput, calls=%fused_computation.85 | convolution fusion | flops 5930745856 | bytes 44598272 | tf_op jit(solution)/shard_map/dot_general | solution.py:230
  534.9 42.9 %reduce-scatter.2.cloned.1.call-done = bf16[256,2048]{1,0:T(8,128)(2,1)} async-done(((bf16[1024,2048]{1,0:T(8,128)(2,1)}), bf16[256,2048]{1,0:T(8,128)(2,1)}) %reduce-scatter.2.cloned.1.call-update) | async-done | bytes 1048592 | tf_op jit(solution)/shard_map/reduce_scatter | solution.py:229
  (350 shorter events, 77.4 us)
Async XLA Ops:
  6.5 5.3 copy-start.2
  6.5 177.9 %all-gather.19.cloned.1.call-start = ((), (), s32[]{:S(2)}) async-start(), calls=%async_computation.8 | async-start | bytes 1179648 | tf_op jit(solution)/shard_map/all_gather | solution.py:14
  118.0 3.5 copy-start.10
  118.0 64.3 %copy-start.5 = (f32[8,128,2]{2,1,0:T(8,128)S(1)}, f32[8,128,2]{2,1,0:T(8,128)}, u32[]{:S(2)}) copy-start(f32[8,128,2]{2,1,0:T(8,128)} %get-tuple-element.228) | copy-start | bytes 24580
  118.0 64.5 %copy-start.4 = (f32[8,128,2]{2,1,0:T(8,128)S(1)}, f32[8,128,2]{2,1,0:T(8,128)}, u32[]{:S(2)}) copy-start(f32[8,128,2]{2,1,0:T(8,128)} %get-tuple-element.235) | copy-start | bytes 24580
  118.7 111.7 %all-gather.11.cloned.1.call-start = ((), (), s32[]{:S(2)}) async-start(), calls=%async_computation.3 | async-start | bytes 10485760 | tf_op jit(solution)/shard_map/all_gather | solution.py:190
  119.5 206.9 %all-gather.13.cloned.1.call-start = ((), (), s32[]{:S(2)}) async-start(), calls=%async_computation.4 | async-start | bytes 6488064 | tf_op jit(solution)/shard_map/all_gather | solution.py:209
  120.2 298.7 %all-gather.15.cloned.1.call-start = ((), (), s32[]{:S(2)}) async-start(), calls=%async_computation.5 | async-start | bytes 6488064 | tf_op jit(solution)/shard_map/all_gather | solution.py:214
  120.8 391.4 %all-gather.17.cloned.1.call-start = ((), (), s32[]{:S(2)}) async-start(), calls=%async_computation.6 | async-start | bytes 6488064 | tf_op jit(solution)/shard_map/all_gather | solution.py:228
  121.4 456.4 %reduce-scatter.2.cloned.1.call-start = ((), (), s32[]{:S(2)}) async-start(), calls=%async_computation.7 | async-start | bytes 5242880 | tf_op jit(solution)/shard_map/reduce_scatter | solution.py:229
  182.5 12.5 %copy-start.3 = (bf16[1024,256]{1,0:T(8,128)(2,1)S(1)}, bf16[1024,256]{1,0:T(8,128)(2,1)}, u32[]{:S(2)}) copy-start(bf16[1024,256]{1,0:T(8,128)(2,1)} %param.21) | copy-start | bytes 1572868
  196.1 2.3 copy-start.9
  200.5 29.9 %copy-start.1 = (bf16[256,2048]{1,0:T(8,128)(2,1)S(1)}, bf16[256,2048]{1,0:T(8,128)(2,1)}, u32[]{:S(2)}) copy-start(bf16[256,2048]{1,0:T(8,128)(2,1)} %param.20) | copy-start | bytes 3145732
  230.5 6.0 %copy-start.8 = (f32[2048]{0:T(1024)S(1)}, f32[2048]{0:T(1024)}, u32[]{:S(2)}) copy-start(f32[2048]{0:T(1024)} %param.30) | copy-start | bytes 24580
  237.4 57.4 %copy-start.6 = (f32[3,1408]{1,0:T(4,128)S(1)}, f32[3,1408]{1,0:T(4,128)}, u32[]{:S(2)}) copy-start(f32[3,1408]{1,0:T(4,128)} %param.34) | copy-start | bytes 50692
  237.4 57.4 %copy-start.7 = (f32[3,1408]{1,0:T(4,128)S(1)}, f32[3,1408]{1,0:T(4,128)}, u32[]{:S(2)}) copy-start(f32[3,1408]{1,0:T(4,128)} %param.33) | copy-start | bytes 50692
  288.2 2.0 copy-start
  290.2 36.2 %collective-permute-start = (bf16[2,2048]{1,0:T(2,128)(2,1)S(1)}, bf16[2,2048]{1,0:T(2,128)(2,1)S(1)}, u32[]{:S(2)}, u32[]{:S(2)}) collective-permute-start(bf16[2,2048]{1,0:T(2,128)(2,1)S(1)} %slice.72), channel_id=1, source_target_pairs={{0,4},{4,8},{8,12},{12,16},{16,20},{20,24},{24,28},{1,5},{5,9},{9,... | collective-permute-start | bytes 24584 | tf_op jit(solution)/shard_map/ppermute | solution.py:35
Sparse Core Ops, SparseCore 0:
  118.8 42.9 all-gather.18
  163.4 66.7 all-gather.10
  232.5 93.8 all-gather.12
  328.4 90.4 all-gather.14
  420.8 91.3 all-gather.16
  535.0 42.7 reduce-scatter.1
